TPU v7x, 128 devices: a whole 4x4x4 slice. The times are simulated.
128 devices in a mesh: rep: 2 (over z_hi), fs: 32 (over z_lo, y, x), tp: 2 (over core).
Axes of the slice: x: 4, y: 4, z: 4 (z_hi: 2, z_lo: 2; z = z_hi * 2 + z_lo), core: 2. Of those that a mesh axis runs over, the one named last changes fastest.
Arguments:
- hidden_in: bfloat16 [40960, 2048], P(('rep', 'fs'), 'tp'), may hold values from -6 to 6
- mix_gain: float32 [2048], replicated, may hold values from 0.1 to 1.9
- w_value: bfloat16 [2048, 1024], P('fs', 'tp'), may hold values from -0.125 to 0.125
- w_gate: bfloat16 [2048, 1024], P('fs', 'tp'), may hold values from -0.125 to 0.125
- conv_taps: float32 [31, 1024], P(None, 'tp'), may hold values from -5 to 5
- conv_bias: float32 [1024], P('tp'), may hold values from -3 to 3
- chan_gain: float32 [1024], P('tp'), may hold values from 0.1 to 1.9
- chan_bias: float32 [1024], P('tp'), may hold values from -3 to 3
- w_back: bfloat16 [1024, 2048], P('tp', 'fs'), may hold values from -0.1875 to 0.1875
- feed_gain: float32 [2048], replicated, may hold values from 0.1 to 1.9
- w_up: bfloat16 [2048, 8192], P(None, ('fs', 'tp')), may hold values from -0.125 to 0.125
- w_down: bfloat16 [8192, 2048], P(('fs', 'tp')), may hold values from -0.0625 to 0.0625
Outputs:
- layer_out: bfloat16 [40960, 2048], P(('rep', 'fs'), 'tp')
All inputs are finite; a program needn't handle non-finite values.
Results may differ from a plain program's by a relative error of at most 0.015.
Values may be sent and summed in bfloat16 or wider, within the bound.
A program may use at most 128 MiB of HBM per device.

v0:
```python
import jax
import jax.numpy as jnp
from jax import lax
from jax.sharding import PartitionSpec as P

KW = 31
LEN = 128


def copy_for_each(array, axis):
    copies = jnp.broadcast_to(array, (lax.axis_size(axis), *array.shape))
    return lax.all_to_all(copies, axis, split_axis=0, concat_axis=0, tiled=True)


def in_order(parts, dim):
    lengths = list(parts.shape[1:])
    lengths[dim] *= parts.shape[0]
    return jnp.moveaxis(parts, 0, dim).reshape(lengths)


def gathered_copies(array, axis, dim):
    parts = copy_for_each(array, axis)
    return in_order(parts, dim)


def side_by_side(arrays, axis, dim, along):
    widths = [a.shape[along] for a in arrays]
    both = jnp.concatenate(arrays, axis=along)
    result = lax.all_gather(both, axis, axis=dim, tiled=True)
    return tuple(jnp.split(result, [sum(widths[:k]) for k in range(1, len(widths))], axis=along))


def in_blocks(array, dim, count):
    lengths = array.shape
    parts = array.reshape(*lengths[:dim], count, lengths[dim] // count, *lengths[dim + 1 :])
    return jnp.moveaxis(parts, dim, 0)


def summed_on_arrival(array, axis, dim):
    count = lax.axis_size(axis)
    parts = lax.all_to_all(in_blocks(array, dim, count), axis, 0, 0, tiled=True)
    return jnp.sum(parts.astype(jnp.float32), axis=0)


def rms_norm(stream, gain):
    values = stream.astype(jnp.float32)
    scaled = values * lax.rsqrt(jnp.mean(values * values, axis=-1, keepdims=True) + 1e-06)
    return (scaled * gain).astype(jnp.bfloat16)


def causal_filter(gated, conv_taps, conv_bias):
    channels = gated.shape[1]
    blocks = gated.reshape(gated.shape[0] // LEN, LEN, channels)
    padded = jnp.pad(blocks, ((0, 0), (KW - 1, 0), (0, 0)))
    result = jnp.zeros_like(blocks) + conv_bias
    for tap_index in range(KW):
        result = result + conv_taps[tap_index] * padded[:, tap_index : tap_index + LEN]
    return result.reshape(gated.shape)


def shards(
    hidden_in,
    mix_gain,
    w_value,
    w_gate,
    conv_taps,
    conv_bias,
    chan_gain,
    chan_bias,
    w_back,
    feed_gain,
    w_up,
    w_down,
):
    gathered = gathered_copies(hidden_in, "tp", 1)
    normed = rms_norm(gathered, mix_gain)
    local_channels = w_value.shape[1]
    whole_value, whole_gate = side_by_side((w_value, w_gate), "fs", 0, 1)
    value_proj = jnp.dot(normed, whole_value, preferred_element_type=jnp.float32)
    gate_proj = jnp.dot(normed, whole_gate, preferred_element_type=jnp.float32)
    gated = value_proj * jax.nn.sigmoid(gate_proj)
    filtered = causal_filter(gated, conv_taps, conv_bias)
    channel_total = local_channels * lax.axis_size("tp")
    first_sum, square_sum = lax.psum(
        (jnp.sum(filtered, axis=1), jnp.sum(filtered * filtered, axis=1)), "tp"
    )
    chan_mean = (first_sum / channel_total)[:, None]
    chan_var = (square_sum / channel_total)[:, None] - chan_mean * chan_mean
    centred = (filtered - chan_mean) * lax.rsqrt(chan_var + 1e-05) * chan_gain + chan_bias
    mixer_act = jax.nn.silu(centred).astype(jnp.bfloat16)
    whole_back = gathered_copies(w_back, "fs", 1)
    partial_value = jnp.dot(mixer_act, whole_back, preferred_element_type=jnp.float32)
    summed = summed_on_arrival(partial_value.astype(jnp.bfloat16), "tp", 1)
    second = (hidden_in.astype(jnp.float32) + summed).astype(jnp.bfloat16)
    gathered_feed = lax.all_gather(second, "tp", axis=1, tiled=True)
    normed_feed = rms_norm(gathered_feed, feed_gain)
    up_proj = jnp.dot(
        normed_feed,
        lax.all_gather(w_up, "fs", axis=1, tiled=True),
        preferred_element_type=jnp.float32,
    )
    hidden = jnp.square(jax.nn.relu(up_proj)).astype(jnp.bfloat16)
    feed_partial = jnp.dot(
        hidden, lax.all_gather(w_down, "fs", axis=0, tiled=True), preferred_element_type=jnp.float32
    )
    feed = summed_on_arrival(feed_partial.astype(jnp.bfloat16), "tp", 1)
    return (second.astype(jnp.float32) + feed).astype(jnp.bfloat16)


def solution(mesh):
    placed = (
        P(("rep", "fs"), "tp"),
        P(),
        P("fs", "tp"),
        P("fs", "tp"),
        P(None, "tp"),
        P("tp"),
        P("tp"),
        P("tp"),
        P("tp", "fs"),
        P(),
        P(None, ("fs", "tp")),
        P(("fs", "tp"), None),
    )
    return jax.shard_map(
        shards, mesh=mesh, in_specs=placed, out_specs=P(("rep", "fs"), "tp"), check_vma=False
    )
```

profile of v0, /device:TPU:1, one launch (start us, length us, event | category | flops | bytes accessed | tf_op | source)
XLA Modules:
  0.0 708.8 jit_solution(11881618682649393780)
XLA Ops:
  6.5 0.0 all-gather.5.cloned.1.call-start
  6.5 1.5 pad_maximum_fusion
  8.1 0.0 all-gather.5.cloned.1.call-update
  8.1 1.7 copy.15
  9.8 0.2 broadcast_in_dim.4
  10.0 0.0 copy-start.5
  10.0 7.0 all_to_all.20
  17.0 1.6 broadcast_in_dim.5
  18.6 8.6 %all-to-all-start.1 = ((bf16[32,512,64]{1,2,0:T(8,128)(2,1)}), bf16[32,512,64]{1,2,0:T(8,128)(2,1)}, u32[]{:S(2)}, u32[]{:S(2)}) async-start(bf16[32,512,64]{1,2,0:T(8,128)(2,1)} %broadcast_in_dim.5), calls=%async_computation.1 | async-start | bytes 4194304 | tf_op jit(solution)/shard_map/all_to_all | solution.py:12
  27.3 0.0 copy-start.6
  27.3 0.0 copy-start.7
  27.3 0.0 all-gather.7.cloned.1.call-start
  27.3 0.6 multiply_reduce_fusion
  27.9 0.2 copy-done.6
  28.2 0.0 copy-done.7
  28.2 2.2 fusion.4
  30.4 127.4 %all-gather.5.cloned.1.call-done = bf16[2048,1024]{1,0:T(8,128)(2,1)} async-done(((bf16[64,1024]{1,0:T(8,128)(2,1)}), bf16[2048,1024]{1,0:T(8,128)(2,1)}) %all-gather.5.cloned.1.call-update) | async-done | bytes 4194320 | tf_op jit(solution)/shard_map/all_gather | solution.py:29
  157.8 4.2 fusion.28
  162.0 0.0 copy-start.8
  162.1 1.6 fusion.16
  163.7 0.0 copy-start.9
  163.7 0.0 copy-start.10
  163.7 5.5 fusion.93
  169.2 22.1 %all-reduce.1 = (f32[640]{0:T(1024)S(1)}, f32[640]{0:T(1024)S(1)}) all-reduce(f32[640]{0:T(1024)S(1)} %bitcast.77, f32[640]{0:T(1024)S(1)} %bitcast.76), channel_id=1, replica_groups=mesh['rep'=2,'fs'=32,'tp'=2] {'tp'}, use_global_device_ids=true, to_apply=%region_4.5 | all-reduce | flops 1280 | bytes 10240 | tf_op jit(solution)/shard_map/psum | solution.py:84
  191.2 0.5 multiply_convert_fusion.1
  191.8 0.0 all-to-all-done.1
  191.8 3.1 convolution_convert_fusion
  194.9 0.3 copy.23
  195.2 5.8 all_to_all.21
  201.0 0.6 convert_reduce_fusion.1
  201.6 0.7 copy-done.2
  202.3 1.5 add_convert_fusion.1
  203.9 0.0 all-gather.7.cloned.1.call-update
  203.9 0.0 all-gather.11.cloned.1.call-start
  204.0 0.7 all-gather.11.cloned.1.call-update
  204.6 0.2 all-gather.9.cloned.1.call-start
  204.9 0.3 all-gather.9.cloned.1.call-update
  205.2 0.0 copy-start.11
  205.2 13.4 %all-gather.7.cloned.1.call-done = bf16[640,2048]{1,0:T(8,128)(2,1)} async-done(((bf16[640,1024]{1,0:T(8,128)(2,1)}), bf16[640,2048]{1,0:T(8,128)(2,1)}) %all-gather.7.cloned.1.call-update) | async-done | bytes 2621456 | tf_op jit(solution)/shard_map/all_gather | solution.py:95
  218.7 2.5 fusion
  221.2 190.3 %all-gather.11.cloned.1.call-done = bf16[4096,2048]{1,0:T(8,128)(2,1)} async-done(((bf16[128,2048]{1,0:T(8,128)(2,1)}), bf16[4096,2048]{1,0:T(8,128)(2,1)}) %all-gather.11.cloned.1.call-update) | async-done | bytes 16777232 | tf_op jit(solution)/shard_map/all_gather | solution.py:104
  411.5 222.9 %all-gather.9.cloned.1.call-done = bf16[2048,4096]{1,0:T(8,128)(2,1)} async-done(((bf16[2048,128]{1,0:T(8,128)(2,1)}), bf16[2048,4096]{1,0:T(8,128)(2,1)}) %all-gather.9.cloned.1.call-update) | async-done | bytes 16777232 | tf_op jit(solution)/shard_map/all_gather | solution.py:99
  634.4 33.8 %convolution_convert_fusion.1 = bf16[640,2048]{1,0:T(8,128)(2,1)} fusion(bf16[4096,2048]{1,0:T(8,128)(2,1)} %all-gather.11.cloned.1.call-done, bf16[2048,4096]{1,0:T(8,128)(2,1)} %all-gather.9.cloned.1.call-done, bf16[640,2048]{1,0:T(8,128)(2,1)S(1)} %copy-done.3, f32[2048]{0:T(1024)S(1)} %copy-done.11, f32[640]{0:T(1024)S(1)} %add_rsqrt_fusion), kind=kOutput, calls=%fused_computation.43 | convolution fusion | flops 21489254400 | bytes 38808064 | tf_op jit(solution)/shard_map/dot_general | solution.py:103
  668.2 2.0 copy.22
  670.2 29.3 %all_to_all.22 = bf16[2,640,1024]{2,1,0:T(8,128)(2,1)S(1)} all-to-all(bf16[2,640,1024]{2,1,0:T(8,128)(2,1)S(1)} %bitcast.71), channel_id=1, replica_groups=mesh['rep'=2,'fs'=32,'tp'=2] {'tp'}, dimensions={0} | all-to-all | bytes 5242880 | tf_op jit(solution)/shard_map/all_to_all | solution.py:41
  699.4 0.6 convert_reduce_fusion
  700.0 0.7 copy-done
  700.8 1.5 add_convert_fusion
  (18 shorter events, 0.1 us)
Async XLA Ops:
  6.5 151.2 %all-gather.5.cloned.1.call-start = ((), (), s32[]{:S(2)}) async-start(), calls=%async_computation.4 | async-start | bytes 4325376 | tf_op jit(solution)/shard_map/all_gather | solution.py:29
  10.0 7.0 copy-start.5
  18.6 173.2 %all-to-all-start.1 = ((bf16[32,512,64]{1,2,0:T(8,128)(2,1)}), bf16[32,512,64]{1,2,0:T(8,128)(2,1)}, u32[]{:S(2)}, u32[]{:S(2)}) async-start(bf16[32,512,64]{1,2,0:T(8,128)(2,1)} %broadcast_in_dim.5), calls=%async_computation.1 | async-start | bytes 4194304 | tf_op jit(solution)/shard_map/all_to_all | solution.py:12
  27.3 0.8 copy-start.6
  27.3 0.9 copy-start.7
  27.3 191.4 %all-gather.7.cloned.1.call-start = ((), (), s32[]{:S(2)}) async-start(), calls=%async_computation.5 | async-start | bytes 3932160 | tf_op jit(solution)/shard_map/all_gather | solution.py:95
  30.4 131.7 %copy-start.1 = (bf16[640,2048]{0,1:T(8,128)(2,1)S(1)}, bf16[640,2048]{0,1:T(8,128)(2,1)}, u32[]{:S(2)}) copy-start(bf16[640,2048]{0,1:T(8,128)(2,1)} %fusion.4) | copy-start | bytes 7864324
  157.8 4.3 copy-start.4
  162.0 1.6 copy-start.8
  163.7 27.6 %copy-start.9 = (f32[512]{0:T(512)S(1)}, f32[512]{0:T(512)}, u32[]{:S(2)}) copy-start(f32[512]{0:T(512)} %param.19) | copy-start | bytes 6148
  163.7 27.6 %copy-start.10 = (f32[512]{0:T(512)S(1)}, f32[512]{0:T(512)}, u32[]{:S(2)}) copy-start(f32[512]{0:T(512)} %param.18) | copy-start | bytes 6148
  201.0 1.3 copy-start.2
  203.9 207.6 %all-gather.11.cloned.1.call-start = ((), (), s32[]{:S(2)}) async-start(), calls=%async_computation.7 | async-start | bytes 17301504 | tf_op jit(solution)/shard_map/all_gather | solution.py:104
  204.6 429.8 %all-gather.9.cloned.1.call-start = ((), (), s32[]{:S(2)}) async-start(), calls=%async_computation.6 | async-start | bytes 17301504 | tf_op jit(solution)/shard_map/all_gather | solution.py:99
  205.2 429.2 %copy-start.11 = (f32[2048]{0:T(1024)S(1)}, f32[2048]{0:T(1024)}, u32[]{:S(2)}) copy-start(f32[2048]{0:T(1024)} %param.21) | copy-start | bytes 24580
  218.7 415.7 %copy-start.3 = (bf16[640,2048]{1,0:T(8,128)(2,1)S(1)}, bf16[640,2048]{1,0:T(8,128)(2,1)}, u32[]{:S(2)}) copy-start(bf16[640,2048]{1,0:T(8,128)(2,1)} %all-gather.7.cloned.1.call-done) | copy-start | bytes 7864324
  699.4 1.3 copy-start
Sparse Core Ops, SparseCore 0:
  9.0 148.7 all-gather.4
  204.0 14.6 all-gather.6
  220.3 191.0 all-gather.10
  412.9 221.4 all-gather.8
where the time goes:
time: 709 us
  waiting for transfers between devices  555 us (78%)
  blocking collectives  64.1 us (9%)
  matrix products  42.7 us (6%)
  other arithmetic  17 us (2%)
  between operations  13.3 us (2%)
  starting transfers between devices  8.94 us (1%)
  local copies, waits for them, and re-layouts  7.52 us (1%)
    all_gather x1, waiting for transfers between devices, shards(): lax.all_gather(w_up, 'fs', axis=1, tiled=True)  223 us
    all_gather x1, waiting for transfers between devices, shards(): lax.all_gather(w_down, 'fs', axis=0, tiled=True)  190 us
    all_gather x1, waiting for transfers between devices, side_by_side(): result = lax.all_gather(both, axis, axis=dim, tiled=True)  127 us
    all_to_all x2, blocking collectives, summed_on_arrival(): parts = lax.all_to_all(in_blocks(array, dim, count), axis, 0, 0, tiled=True)  35.1 us
    dot_general x1, matrix products, shards(): jnp.dot(hidden, lax.all_gather(w_down, 'fs', axis=0, tiled=True), preferr...  33.8 us
    psum x1, blocking collectives, shards(): lax.psum((jnp.sum(filtered, axis=1), jnp.sum(filtered * filtered, axis=1)...  22.1 us
  transfers between devices with their start and end apart: 5, of which 4 were waited for; matrix products, arithmetic and copies ran while one was open for 3% of the time, Pallas kernels for 0%

commit v1 on v0

--- a/solution.py
+++ b/solution.py
@@ -96,7 +96,7 @@
     normed_feed = rms_norm(gathered_feed, feed_gain)
     up_proj = jnp.dot(
         normed_feed,
-        lax.all_gather(w_up, "fs", axis=1, tiled=True),
+        jnp.concatenate(lax.all_gather(w_up, "fs"), axis=1),
         preferred_element_type=jnp.float32,
     )
     hidden = jnp.square(jax.nn.relu(up_proj)).astype(jnp.bfloat16)

time: 709 us -> 635 us (0.90)
  waiting for transfers between devices: 555 us -> 485 us
  blocking collectives: 64.1 us -> 41.3 us
  local copies, waits for them, and re-layouts: 7.52 us -> 27.2 us
    all_gather x1, waiting for transfers between devices: 190 us -> 153 us  [shards(): lax.all_gather(w_down, 'fs', axis=0, tiled=True)]
    all_gather x1, waiting for transfers between devices: 223 us -> 190 us  [shards(): lax.all_gather(w_up, 'fs')]
    all_to_all x2, blocking collectives: 35.1 us -> 12.3 us  [summed_on_arrival(): parts = lax.all_to_all(in_blocks(array, dim, count), axis, 0, 0, tiled=True)]
    reshape x0 -> x1, local copies, waits for them, and re-layouts: none -> 21.5 us  [shards(): jnp.concatenate(lax.all_gather(w_up, 'fs'), axis=1)]
    dot_general x1, matrix products: 33.8 us -> 16 us  [shards(): jnp.dot(hidden, lax.all_gather(w_down, 'fs', axis=0, tiled=True), preferr...]
    dot_general x0 -> x1, matrix products: none -> 16.3 us  [shards(): jnp.dot(normed_feed, jnp.concatenate(lax.all_gather(w_up, 'fs'), axis=1),...]
  transfers between devices with their start and end apart: 5 -> 5, of which waited for: 4 -> 4; matrix products, arithmetic and copies ran while one was open for 3% -> 9% of each run, Pallas kernels for 0% -> 0%
where the time goes in v1:
time: 635 us; the launch traced here: 634 us
  waiting for transfers between devices  485 us (76%)
  matrix products  41.4 us (7%)
  blocking collectives  41.3 us (7%)
  local copies, waits for them, and re-layouts  27.2 us (4%)
  other arithmetic  16.9 us (3%)
  between operations  13.3 us (2%)
  starting transfers between devices  8.94 us (1%)
    all_gather x1, waiting for transfers between devices, shards(): lax.all_gather(w_up, 'fs')  190 us
    all_gather x1, waiting for transfers between devices, shards(): lax.all_gather(w_down, 'fs', axis=0, tiled=True)  153 us
    all_gather x1, waiting for transfers between devices, side_by_side(): result = lax.all_gather(both, axis, axis=dim, tiled=True)  127 us
    psum x1, blocking collectives, shards(): lax.psum((jnp.sum(filtered, axis=1), jnp.sum(filtered * filtered, axis=1)...  22.1 us
    reshape x1, local copies, waits for them, and re-layouts, shards(): jnp.concatenate(lax.all_gather(w_up, 'fs'), axis=1)  21.5 us
    dot_general x1, matrix products, shards(): jnp.dot(normed_feed, jnp.concatenate(lax.all_gather(w_up, 'fs'), axis=1),...  16.3 us
    dot_general x1, matrix products, shards(): jnp.dot(hidden, lax.all_gather(w_down, 'fs', axis=0, tiled=True), preferr...  16 us
    all_gather x1, waiting for transfers between devices, shards(): gathered_feed = lax.all_gather(second, 'tp', axis=1, tiled=True)  13.5 us
  transfers between devices with their start and end apart: 5, of which 4 were waited for; matrix products, arithmetic and copies ran while one was open for 9% of the time, Pallas kernels for 0%

profile of v1, /device:TPU:1, one launch (start us, length us, event | category | flops | bytes accessed | tf_op | source)
XLA Modules:
  0.0 634.3 jit_solution(14717275180474212320)
XLA Ops:
  6.5 0.0 all-gather.6.cloned.1.call-start
  6.5 1.5 pad_maximum_fusion
  8.1 0.0 all-gather.6.cloned.1.call-update
  8.1 1.7 copy.17
  9.8 0.2 broadcast_in_dim.4
  10.0 0.0 copy-start.5
  10.0 7.0 %all_to_all.20 = bf16[2,640,1024]{1,2,0:T(8,128)(2,1)S(1)} all-to-all(bf16[2,640,1024]{1,2,0:T(8,128)(2,1)S(1)} %broadcast_in_dim.4), channel_id=1, replica_groups=mesh['rep'=2,'fs'=32,'tp'=2] {'tp'}, dimensions={0} | all-to-all | bytes 5242880 | tf_op jit(solution)/shard_map/all_to_all | solution.py:12
  17.0 1.6 broadcast_in_dim.5
  18.6 8.6 %all-to-all-start.1 = ((bf16[32,512,64]{1,2,0:T(8,128)(2,1)}), bf16[32,512,64]{1,2,0:T(8,128)(2,1)}, u32[]{:S(2)}, u32[]{:S(2)}) async-start(bf16[32,512,64]{1,2,0:T(8,128)(2,1)} %broadcast_in_dim.5), calls=%async_computation.1 | async-start | bytes 4194304 | tf_op jit(solution)/shard_map/all_to_all | solution.py:12
  27.3 0.0 copy-start.6
  27.3 0.0 copy-start.7
  27.3 0.0 all-gather.8.cloned.1.call-start
  27.3 0.6 multiply_reduce_fusion
  27.9 0.2 copy-done.6
  28.2 2.2 fusion.4
  30.4 127.4 %all-gather.6.cloned.1.call-done = bf16[2048,1024]{1,0:T(8,128)(2,1)} async-done(((bf16[64,1024]{1,0:T(8,128)(2,1)}), bf16[2048,1024]{1,0:T(8,128)(2,1)}) %all-gather.6.cloned.1.call-update) | async-done | bytes 4194320 | tf_op jit(solution)/shard_map/all_gather | solution.py:29
  157.8 4.2 fusion.28
  162.0 0.0 copy-start.8
  162.1 1.6 fusion.16
  163.7 0.0 copy-start.9
  163.7 0.0 copy-start.10
  163.7 5.5 fusion.93
  169.2 22.1 %all-reduce.1 = (f32[640]{0:T(1024)S(1)}, f32[640]{0:T(1024)S(1)}) all-reduce(f32[640]{0:T(1024)S(1)} %bitcast.88, f32[640]{0:T(1024)S(1)} %bitcast.87), channel_id=1, replica_groups=mesh['rep'=2,'fs'=32,'tp'=2] {'tp'}, use_global_device_ids=true, to_apply=%region_4.5 | all-reduce | flops 1280 | bytes 10240 | tf_op jit(solution)/shard_map/psum | solution.py:84
  191.2 0.5 multiply_convert_fusion.1
  191.8 0.0 all-to-all-done.1
  191.8 3.1 convolution_convert_fusion
  194.9 0.3 copy.26
  195.2 5.8 all_to_all.21
  201.0 0.6 convert_reduce_fusion.1
  201.6 0.7 copy-done.2
  202.3 1.5 add_convert_fusion.1
  203.9 0.0 all-gather.8.cloned.1.call-update
  203.9 0.0 all-gather.12.cloned.1.call-start
  204.0 0.7 all-gather.12.cloned.1.call-update
  204.6 0.2 all-gather.10.cloned.1.call-start
  204.9 0.3 all-gather.10.cloned.1.call-update
  205.2 13.5 %all-gather.8.cloned.1.call-done = bf16[640,2048]{1,0:T(8,128)(2,1)} async-done(((bf16[640,1024]{1,0:T(8,128)(2,1)}), bf16[640,2048]{1,0:T(8,128)(2,1)}) %all-gather.8.cloned.1.call-update) | async-done | bytes 2621456 | tf_op jit(solution)/shard_map/all_gather | solution.py:95
  218.7 2.3 fusion
  221.0 190.5 %all-gather.12.cloned.1.call-done = bf16[65536,128]{1,0:T(8,128)(2,1)} async-done(((bf16[2048,128]{1,0:T(8,128)(2,1)}), bf16[65536,128]{1,0:T(8,128)(2,1)}) %all-gather.12.cloned.1.call-update) | async-done | bytes 16777232 | tf_op jit(solution)/shard_map/all_gather | solution.py:99
  411.5 21.5 %copy.19 = bf16[2048,32,128]{0,2,1:T(8,128)(2,1)} copy(bf16[2048,32,128]{2,0,1:T(8,128)(2,1)} %bitcast.79) | data formatting | bytes 33554432 | tf_op jit(solution)/shard_map/reshape | solution.py:99
  432.9 16.3 %multiply_convert_fusion.clone.4 = bf16[640,4096]{1,0:T(8,128)(2,1)} fusion(bf16[2048,4096]{0,1:T(8,128)(2,1)} %bitcast.80, bf16[640,2048]{1,0:T(8,128)(2,1)S(1)} %copy-done.3, f32[2048]{0:T(1024)S(1)} %copy-done.11, f32[640]{0:T(1024)S(1)} %add_rsqrt_fusion), kind=kOutput, calls=%fused_computation.clone.clone.clone.1 | convolution fusion | flops 10750525440 | bytes 24652288 | tf_op jit(solution)/shard_map/dot_general | solution.py:97
  449.3 152.8 %all-gather.10.cloned.1.call-done = bf16[4096,2048]{1,0:T(8,128)(2,1)} async-done(((bf16[128,2048]{1,0:T(8,128)(2,1)}), bf16[4096,2048]{1,0:T(8,128)(2,1)}) %all-gather.10.cloned.1.call-update) | async-done | bytes 16777232 | tf_op jit(solution)/shard_map/all_gather | solution.py:104
  602.1 16.0 %convolution_convert_fusion.1 = bf16[640,2048]{1,0:T(8,128)(2,1)S(1)} fusion(bf16[4096,2048]{1,0:T(8,128)(2,1)} %all-gather.10.cloned.1.call-done, bf16[640,4096]{1,0:T(8,128)(2,1)} %multiply_convert_fusion.clone.4), kind=kOutput, calls=%fused_computation.43 | convolution fusion | flops 10738728960 | bytes 24641536 | tf_op jit(solution)/shard_map/dot_general | solution.py:103
  618.1 0.3 copy.25
  618.4 6.5 %all_to_all.22 = bf16[2,640,1024]{2,1,0:T(8,128)(2,1)S(1)} all-to-all(bf16[2,640,1024]{2,1,0:T(8,128)(2,1)S(1)} %bitcast.82), channel_id=1, replica_groups=mesh['rep'=2,'fs'=32,'tp'=2] {'tp'}, dimensions={0} | all-to-all | bytes 5242880 | tf_op jit(solution)/shard_map/all_to_all | solution.py:41
  624.9 0.6 convert_reduce_fusion
  625.5 0.7 copy-done
  626.2 1.5 add_convert_fusion
  (20 shorter events, 0.1 us)
Async XLA Ops:
  6.5 151.2 %all-gather.6.cloned.1.call-start = ((), (), s32[]{:S(2)}) async-start(), calls=%async_computation.4 | async-start | bytes 4325376 | tf_op jit(solution)/shard_map/all_gather | solution.py:29
  10.0 7.0 %copy-start.5 = (bf16[512,64]{0,1:T(8,128)(2,1)S(1)}, bf16[512,64]{0,1:T(8,128)(2,1)}, u32[]{:S(2)}) copy-start(bf16[512,64]{0,1:T(8,128)(2,1)} %param.20) | copy-start | bytes 196612
  18.6 173.2 %all-to-all-start.1 = ((bf16[32,512,64]{1,2,0:T(8,128)(2,1)}), bf16[32,512,64]{1,2,0:T(8,128)(2,1)}, u32[]{:S(2)}, u32[]{:S(2)}) async-start(bf16[32,512,64]{1,2,0:T(8,128)(2,1)} %broadcast_in_dim.5), calls=%async_computation.1 | async-start | bytes 4194304 | tf_op jit(solution)/shard_map/all_to_all | solution.py:12
  27.3 0.8 copy-start.6
  27.3 0.9 copy-start.7
  27.3 191.4 %all-gather.8.cloned.1.call-start = ((), (), s32[]{:S(2)}) async-start(), calls=%async_computation.5 | async-start | bytes 3932160 | tf_op jit(solution)/shard_map/all_gather | solution.py:95
  30.4 131.7 %copy-start.1 = (bf16[640,2048]{0,1:T(8,128)(2,1)S(1)}, bf16[640,2048]{0,1:T(8,128)(2,1)}, u32[]{:S(2)}) copy-start(bf16[640,2048]{0,1:T(8,128)(2,1)} %fusion.4) | copy-start | bytes 7864324
  157.8 4.3 copy-start.4
  162.0 1.6 copy-start.8
  163.7 27.6 %copy-start.9 = (f32[512]{0:T(512)S(1)}, f32[512]{0:T(512)}, u32[]{:S(2)}) copy-start(f32[512]{0:T(512)} %param.19) | copy-start | bytes 6148
  163.7 27.6 %copy-start.10 = (f32[512]{0:T(512)S(1)}, f32[512]{0:T(512)}, u32[]{:S(2)}) copy-start(f32[512]{0:T(512)} %param.18) | copy-start | bytes 6148
  201.0 1.3 copy-start.2
  203.9 207.6 %all-gather.12.cloned.1.call-start = ((), (), s32[]{:S(2)}) async-start(), calls=%async_computation.7 | async-start | bytes 17301504 | tf_op jit(solution)/shard_map/all_gather | solution.py:99
  204.6 397.4 %all-gather.10.cloned.1.call-start = ((), (), s32[]{:S(2)}) async-start(), calls=%async_computation.6 | async-start | bytes 17301504 | tf_op jit(solution)/shard_map/all_gather | solution.py:104
  411.5 21.5 %copy-start.3 = (bf16[640,2048]{1,0:T(8,128)(2,1)S(1)}, bf16[640,2048]{1,0:T(8,128)(2,1)}, u32[]{:S(2)}) copy-start(bf16[640,2048]{1,0:T(8,128)(2,1)} %all-gather.8.cloned.1.call-done) | copy-start | bytes 7864324
  411.5 21.5 %copy-start.11 = (f32[2048]{0:T(1024)S(1)}, f32[2048]{0:T(1024)}, u32[]{:S(2)}) copy-start(f32[2048]{0:T(1024)} %param.21) | copy-start | bytes 24580
  624.9 1.3 copy-start
Sparse Core Ops, SparseCore 0:
  9.0 148.7 all-gather.5
  204.0 14.6 all-gather.7
  220.3 191.0 all-gather.11
  413.0 189.0 all-gather.9
